TPU v7x, 512 devices: a whole 4x8x8 slice. The times are simulated.
512 devices in a mesh: ep: 32 (over z, x), tp: 16 (over y, core).
Axes of the slice: x: 4, y: 8, z: 8, core: 2. Of those that a mesh axis runs over, the one named last changes fastest.
Arguments:
- tokens: bfloat16 [1024, 2048], P(('ep', 'tp')), may hold values from -6 to 6
- cache_keys: bfloat16 [1024, 1024, 256], P(('ep', 'tp')), may hold values from -360 to 360
- cache_values: bfloat16 [1024, 1024, 256], P(('ep', 'tp')), may hold values from -6 to 6
- cache_gates: float32 [1024, 2, 1024], P(('ep', 'tp')), may hold values from -256 to 0, as said below
- lengths: int32 [1024], P(('ep', 'tp')), may hold values from 1 to 1024, 524288 in all
- routes: int32 [1024, 4], P(('ep', 'tp')), may hold values from 0 to 31, all different within a row; in each aligned block of 2 rows (0 to 1, 2 to 3, ...) no two rows name the same one
- route_logits: float32 [1024, 4], P(('ep', 'tp')), may hold values from -6 to 6
- attn_gain: float32 [2048], replicated, may hold values from 0.1 to 1.9
- w_query: bfloat16 [2048, 2048], P(None, 'tp'), may hold values from -0.125 to 0.125
- w_keyval: bfloat16 [2048, 512], P(None, 'tp'), may hold values from -0.125 to 0.125
- w_forget: bfloat16 [2048, 2], replicated, may hold values from -0.125 to 0.125
- forget_bias: float32 [2], replicated, may hold values from -1 to 3
- w_out: bfloat16 [2048, 2048], P(None, 'tp'), may hold values from -0.125 to 0.125
- mix_gain: float32 [2048], replicated, may hold values from 0.1 to 1.9
- ffn_gain: float32 [2048], replicated, may hold values from 0.1 to 1.9
- w_gate: bfloat16 [32, 2048, 2048], P('ep', None, 'tp'), may hold values from -0.125 to 0.125
- w_lin: bfloat16 [32, 2048, 2048], P('ep', None, 'tp'), may hold values from -0.125 to 0.125
- gate_bias: float32 [32, 2048], P('ep', 'tp'), may hold values from -12 to 12
- lin_bias: float32 [32, 2048], P('ep', 'tp'), may hold values from -12 to 12
- w_down: bfloat16 [32, 2048, 2048], P('ep', 'tp'), may hold values from -0.125 to 0.125
- post_gain: float32 [2048], replicated, may hold values from 0.1 to 1.9
Outputs:
- updated: bfloat16 [1024, 2048], P(('ep', 'tp'))
- new_entries: bfloat16 [1024, 512], P(('ep', 'tp'))
Inputs may be any that keep to these rules, and one draw needn't show every extreme that they name: `cache_gates`: along the positions of each sequence and head the values never increase. The lengths of all sequences add up to 524288, and some sequence has exactly 1024. `routes`: each row names 4 different experts; among the rows of one device no expert is named twice; every expert is named by some row.
All inputs are finite; a program needn't handle non-finite values. No bound on the sum of `lengths` on one device may be relied on, other than what follows from the above.
Results may differ from a plain program's by a relative error of at most 0.014.
The roundings to bfloat16 on the way count: a program that leaves them out, or rounds other values in their place, can miss the bound.
Values may be sent and summed in bfloat16 or wider, within the bound.
A program may use at most 64 MiB of HBM per device.

v0:
```python
import jax
import jax.numpy as jnp
from jax import lax
from jax.sharding import PartitionSpec as P

HEADS = 16
KVH = 2
HDIM = 128
NORM_EPS = 1e-06
SWIGLU_ALPHA = 1.702
SWIGLU_LIMIT = 7.0
NEG_LARGE = -1e30


def laid_out(tiles, dim):
    shape = list(tiles.shape[1:])
    shape[dim] *= tiles.shape[0]
    return jnp.moveaxis(tiles, 0, dim).reshape(shape)


def sent_to_all(array, axis):
    copies = jnp.broadcast_to(array, (lax.axis_size(axis), *array.shape))
    return lax.all_to_all(copies, axis, split_axis=0, concat_axis=0, tiled=True)


def gather_directly(array, axis, dim):
    return laid_out(sent_to_all(array, axis), dim)


def rms_scale(values, gain):
    values = values.astype(jnp.float32)
    return values * lax.rsqrt(jnp.mean(values * values, axis=-1, keepdims=True) + NORM_EPS) * gain


def clamped_unit(gate, linear):
    gate = jnp.minimum(gate, SWIGLU_LIMIT)
    linear = jnp.clip(linear, -SWIGLU_LIMIT, SWIGLU_LIMIT)
    return gate * jax.nn.sigmoid(SWIGLU_ALPHA * gate) * (linear + 1.0)


def block_scores(q_four, cache_keys, cache_gates, base, lengths, span, scale):
    seqs = cache_keys.shape[0]
    k_four = cache_keys.reshape(seqs, span, q_four.shape[1], q_four.shape[3])
    scores = (
        jnp.einsum("sgqd,spgd->sgqp", q_four, k_four, preferred_element_type=jnp.float32) * scale
    )
    scores = scores + (base[:, :, None, None] - cache_gates[:, :, None, :])
    place = lax.iota(jnp.int32, span)
    live = place[None, None, None, :] < lengths[:, None, None, None]
    return (jnp.where(live, scores, NEG_LARGE), live)


def per_device(
    tokens,
    cache_keys,
    cache_values,
    cache_gates,
    lengths,
    routes,
    route_logits,
    attn_gain,
    w_query,
    w_keyval,
    w_forget,
    forget_bias,
    w_out,
    mix_gain,
    ffn_gain,
    w_gate,
    w_lin,
    gate_bias,
    lin_bias,
    w_down,
    post_gain,
):
    seqs, width = tokens.shape
    normed = rms_scale(tokens, attn_gain).astype(jnp.bfloat16)
    query_cols = w_query.shape[1]
    pair_cols = w_keyval.shape[1]
    piece = gather_directly(normed, "tp", 0)
    both = jnp.concatenate(
        [
            jnp.dot(piece, w_query, preferred_element_type=jnp.float32),
            jnp.dot(piece, w_keyval, preferred_element_type=jnp.float32),
        ],
        axis=1,
    )
    gathered = both.astype(jnp.bfloat16)
    owned = lax.all_to_all(gathered, "tp", split_axis=0, concat_axis=1, tiled=True)
    groups = lax.axis_size("tp")
    owned = owned.reshape(seqs, groups, query_cols + pair_cols)
    query = owned[:, :, :query_cols].reshape(seqs, groups * query_cols)
    fresh = owned[:, :, query_cols:].reshape(seqs, groups * pair_cols)
    forget = jax.nn.log_sigmoid(
        jnp.dot(normed, w_forget, preferred_element_type=jnp.float32) + forget_bias
    )
    q_four = query.reshape(seqs, KVH, HEADS // KVH, HDIM)
    new_key = fresh[:, : KVH * HDIM].reshape(seqs, KVH, HDIM)
    new_value = fresh[:, KVH * HDIM :].reshape(seqs, KVH, HDIM)
    span_all = cache_keys.shape[1]
    place = lax.iota(jnp.int32, span_all)
    last = jnp.sum(
        jnp.where(place[None, None, :] == lengths[:, None, None] - 1, cache_gates, 0.0), axis=2
    )
    base = last + forget
    scale = HDIM ** (-0.5)
    own = jnp.einsum("sgqd,sgd->sgq", q_four, new_key, preferred_element_type=jnp.float32) * scale
    values_four = cache_values.reshape(seqs, span_all, KVH, HDIM)
    masked, live = block_scores(q_four, cache_keys, cache_gates, base, lengths, span_all, scale)
    top = jnp.maximum(jnp.max(masked, axis=-1), own)
    expo = jnp.where(live, jnp.exp(masked - top[..., None]), 0.0)
    own_expo = jnp.exp(own - top)
    total = jnp.sum(expo, axis=-1) + own_expo
    weights = (expo / total[..., None]).astype(jnp.bfloat16)
    mixed = jnp.einsum("sgqp,spgd->sgqd", weights, values_four, preferred_element_type=jnp.float32)
    own_weight = (own_expo / total).astype(jnp.bfloat16)
    mixed = (
        mixed
        + own_weight.astype(jnp.float32)[..., None] * new_value.astype(jnp.float32)[:, :, None, :]
    )
    mixed = mixed.reshape(seqs, HEADS * HDIM).astype(jnp.bfloat16)
    projected = jnp.dot(
        gather_directly(mixed, "tp", 0), w_out, preferred_element_type=jnp.float32
    ).astype(jnp.bfloat16)
    projected = lax.all_to_all(projected, "tp", split_axis=0, concat_axis=1, tiled=True)
    residual = tokens.astype(jnp.float32) + rms_scale(projected, mix_gain)
    expert_in = rms_scale(residual, ffn_gain).astype(jnp.bfloat16)
    experts = lax.axis_size("ep")
    hit = (routes[:, :, None] == lax.iota(jnp.int32, experts)[None, None, :]).astype(jnp.float32)
    probs = jax.nn.softmax(route_logits, axis=-1)
    combine = jnp.sum(probs[:, :, None] * hit, axis=1)
    chosen = jnp.sum(hit, axis=1).T
    outbound = jnp.dot(
        chosen.astype(jnp.bfloat16), expert_in, preferred_element_type=jnp.float32
    ).astype(jnp.bfloat16)[:, None, :]
    slots = outbound.shape[1]
    arrived = lax.all_to_all(outbound, "ep", split_axis=0, concat_axis=0, tiled=True)
    flat = arrived.reshape(experts * slots, width)
    pooled = lax.all_gather(flat, "tp", axis=0, tiled=True)
    piece = pooled
    gate = jnp.dot(piece, w_gate[0], preferred_element_type=jnp.float32) + gate_bias[0]
    linear = jnp.dot(piece, w_lin[0], preferred_element_type=jnp.float32) + lin_bias[0]
    act = clamped_unit(gate, linear).astype(jnp.bfloat16)
    summed = lax.psum_scatter(
        jnp.dot(act, w_down[0], preferred_element_type=jnp.float32).astype(jnp.bfloat16),
        "tp",
        scatter_dimension=0,
        tiled=True,
    )
    returned = lax.all_to_all(
        summed.reshape(experts, slots, width), "ep", split_axis=0, concat_axis=0, tiled=True
    )
    moe = jnp.einsum("se,ed->sd", combine, returned[:, 0, :].astype(jnp.float32))
    updated = (residual + rms_scale(moe, post_gain)).astype(jnp.bfloat16)
    return (updated, fresh)


def solution(mesh):
    in_specs = (
        P(("ep", "tp"), None),
        P(("ep", "tp"), None, None),
        P(("ep", "tp"), None, None),
        P(("ep", "tp"), None, None),
        P(("ep", "tp")),
        P(("ep", "tp"), None),
        P(("ep", "tp"), None),
        P(),
        P(None, "tp"),
        P(None, "tp"),
        P(),
        P(),
        P(None, "tp"),
        P(),
        P(),
        P("ep", None, "tp"),
        P("ep", None, "tp"),
        P("ep", "tp"),
        P("ep", "tp"),
        P("ep", "tp", None),
        P(),
    )
    out_specs = (P(("ep", "tp"), None), P(("ep", "tp"), None))
    return jax.shard_map(
        per_device, mesh=mesh, in_specs=in_specs, out_specs=out_specs, check_vma=False
    )
```

profile of v0, /device:TPU:25, one launch (start us, length us, event | category | flops | bytes accessed | tf_op | source)
XLA Modules:
  0.0 220.4 jit_solution(12834729480745042205)
XLA Ops:
  7.2 0.0 copy-start
  7.2 1.0 fusion.67
  8.2 0.8 fusion.69
  9.0 0.7 broadcast_in_dim.37
  9.7 9.2 %all-to-all-start = ((bf16[16,2,2048]{2,1,0:T(2,128)(2,1)}), bf16[16,2,2048]{2,1,0:T(2,128)(2,1)S(1)}, u32[]{:S(2)}, u32[]{:S(2)}) async-start(bf16[16,2,2048]{2,1,0:T(2,128)(2,1)} %broadcast_in_dim.37), calls=%async_computation | async-start | bytes 262144 | tf_op jit(solution)/shard_map/all_to_all | solution.py:23
  18.9 0.7 broadcast_add_fusion
  19.5 0.1 iota_compare_fusion
  19.6 0.8 select_reduce_fusion
  20.4 0.8 fusion.77
  21.3 0.8 broadcast_subtract_fusion
  22.1 3.2 %all-to-all-done = bf16[16,2,2048]{2,1,0:T(2,128)(2,1)S(1)} async-done(((bf16[16,2,2048]{2,1,0:T(2,128)(2,1)}), bf16[16,2,2048]{2,1,0:T(2,128)(2,1)S(1)}, u32[]{:S(2)}, u32[]{:S(2)}) %all-to-all-start) | async-done | bytes 131104 | tf_op jit(solution)/shard_map/all_to_all | solution.py:23
  25.2 1.1 convolution_convert_fusion.3
  26.3 0.0 copy-start.4
  26.3 1.3 convolution_convert_fusion.4
  27.6 0.0 copy-start.2
  27.6 0.6 copy.45
  28.2 5.8 %all-to-all-start.1 = ((bf16[16,2,160]{2,1,0:T(2,128)(2,1)}), bf16[16,2,160]{2,1,0:T(2,128)(2,1)S(1)}, u32[]{:S(2)}, u32[]{:S(2)}) async-start(bf16[16,2,160]{2,1,0:T(2,128)(2,1)} %copy.45), calls=%async_computation.1 | async-start | bytes 32768 | tf_op jit(solution)/shard_map/all_to_all | solution.py:89
  34.0 0.7 iota_compare_fusion.1
  34.7 0.8 reduce_max.19
  35.5 3.0 %all-to-all-done.1 = bf16[16,2,160]{2,1,0:T(2,128)(2,1)S(1)} async-done(((bf16[16,2,160]{2,1,0:T(2,128)(2,1)}), bf16[16,2,160]{2,1,0:T(2,128)(2,1)S(1)}, u32[]{:S(2)}, u32[]{:S(2)}) %all-to-all-start.1) | async-done | bytes 10272 | tf_op jit(solution)/shard_map/all_to_all | solution.py:89
  38.5 0.1 reshape.145
  38.7 0.1 fusion.70
  38.8 0.0 copy-start.5
  38.8 0.5 fusion.88
  39.3 0.2 fusion.59
  39.5 0.0 copy-start.10
  39.5 0.3 fusion.31
  39.9 0.7 broadcast_in_dim.42
  40.6 6.6 %all-to-all-start.2 = ((bf16[16,2,2048]{2,1,0:T(2,128)(2,1)}), bf16[16,2,2048]{2,1,0:T(2,128)(2,1)S(1)}, u32[]{:S(2)}, u32[]{:S(2)}) async-start(bf16[16,2,2048]{2,1,0:T(2,128)(2,1)} %broadcast_in_dim.42), calls=%async_computation.2 | async-start | bytes 262144 | tf_op jit(solution)/shard_map/all_to_all | solution.py:23
  47.1 0.0 copy-done.4
  47.1 0.2 fusion.80
  47.3 0.1 fusion.79
  47.4 6.1 %all-to-all-done.2 = bf16[16,2,2048]{2,1,0:T(2,128)(2,1)S(1)} async-done(((bf16[16,2,2048]{2,1,0:T(2,128)(2,1)}), bf16[16,2,2048]{2,1,0:T(2,128)(2,1)S(1)}, u32[]{:S(2)}, u32[]{:S(2)}) %all-to-all-start.2) | async-done | bytes 131104 | tf_op jit(solution)/shard_map/all_to_all | solution.py:23
  53.5 0.1 reshape.148
  53.6 0.8 convolution_convert_fusion.2
  54.4 5.7 %all-to-all-start.3 = ((bf16[16,2,128]{2,1,0:T(2,128)(2,1)}), bf16[16,2,128]{2,1,0:T(2,128)(2,1)S(1)}, u32[]{:S(2)}, u32[]{:S(2)}) async-start(bf16[16,2,128]{2,1,0:T(2,128)(2,1)} %bitcast.6), calls=%async_computation.3 | async-start | bytes 16384 | tf_op jit(solution)/shard_map/all_to_all | solution.py:125
  60.1 0.0 all-gather.3.cloned.1.call-start
  60.1 0.0 copy-done.9
  60.1 0.1 convert_reduce_fusion
  60.2 4.0 %all-to-all-done.3 = bf16[16,2,128]{2,1,0:T(2,128)(2,1)S(1)} async-done(((bf16[16,2,128]{2,1,0:T(2,128)(2,1)}), bf16[16,2,128]{2,1,0:T(2,128)(2,1)S(1)}, u32[]{:S(2)}, u32[]{:S(2)}) %all-to-all-start.3) | async-done | bytes 8224 | tf_op jit(solution)/shard_map/all_to_all | solution.py:125
  64.2 0.1 fusion.66
  64.4 0.0 copy-done.8
  64.4 0.2 multiply_reduce_fusion.1
  64.6 0.2 fusion
  64.9 0.5 broadcast.126
  65.4 0.7 reduce.2
  66.0 0.1 reshape.160
  66.1 0.0 copy-start.11
  66.1 20.5 %all_to_all.46 = bf16[32,2,1024]{2,1,0:T(2,128)(2,1)S(1)} all-to-all(bf16[32,2,1024]{2,1,0:T(2,128)(2,1)S(1)} %reshape.160), channel_id=1, replica_groups=mesh['ep'=32,'tp'=16] {'ep'}, dimensions={0} | all-to-all | bytes 262144 | tf_op jit(solution)/shard_map/all_to_all | solution.py:137
  86.6 0.1 reshape.161
  86.7 0.7 copy.51
  87.4 0.0 all-gather.3.cloned.1.call-update
  87.5 0.0 reduce-scatter.2.cloned.1.call-start
  87.5 36.1 %all-gather.3.cloned.1.call-done = bf16[512,1,2048]{2,0,1:T(8,128)(2,1)} async-done(((bf16[32,1,2048]{2,0,1:T(8,128)(2,1)}), bf16[512,1,2048]{2,0,1:T(8,128)(2,1)}) %all-gather.3.cloned.1.call-update) | async-done | bytes 2097168 | tf_op jit(solution)/shard_map/all_gather | solution.py:139
  123.7 2.5 %fusion.8 = f32[512,128]{1,0:T(8,128)S(1)} fusion(bf16[512,1,2048]{2,0,1:T(8,128)(2,1)} %all-gather.3.cloned.1.call-done, bf16[1,2048,128]{2,1,0:T(8,128)(2,1)} %param.36, f32[128]{0:T(128)S(1)} %bitcast.104), kind=kOutput, calls=%fused_computation.8 | convolution fusion | flops 268566528 | bytes 2884096 | tf_op jit(solution)/shard_map/dot_general | solution.py:141
  126.2 3.8 %convolution_convert_fusion = bf16[512,2048]{1,0:T(8,128)(2,1)} fusion(bf16[512,1,2048]{2,0,1:T(8,128)(2,1)S(1)} %copy-done.1, bf16[1,128,2048]{2,1,0:T(8,128)(2,1)} %param.40, bf16[1,2048,128]{2,1,0:T(8,128)(2,1)} %param.37, f32[512,128]{1,0:T(8,128)S(1)} %fusion.8, f32[128]{0:T(128)S(1)} %bitcast.105), kind=kOutput, calls=%fused_computation | convolution fusion | flops 538574848 | bytes 5505536 | tf_op jit(solution)/shard_map/dot_general | solution.py:145
  130.0 0.0 reduce-scatter.2.cloned.1.call-update
  130.1 61.4 %reduce-scatter.2.cloned.1.call-done = bf16[32,2048]{1,0:T(8,128)(2,1)} async-done(((bf16[512,2048]{1,0:T(8,128)(2,1)}), bf16[32,2048]{1,0:T(8,128)(2,1)}) %reduce-scatter.2.cloned.1.call-update) | async-done | bytes 131088 | tf_op jit(solution)/shard_map/reduce_scatter | solution.py:144
  191.5 1.6 reduce.3
  193.1 0.1 reshape.162
  193.1 19.3 %all_to_all.47 = bf16[32,2,1024]{2,1,0:T(2,128)(2,1)S(1)} all-to-all(bf16[32,2,1024]{2,1,0:T(2,128)(2,1)S(1)} %reshape.162), channel_id=1, replica_groups=mesh['ep'=32,'tp'=16] {'ep'}, dimensions={0} | all-to-all | bytes 262144 | tf_op jit(solution)/shard_map/all_to_all | solution.py:150
  212.5 0.1 reshape.163
  212.6 0.3 multiply_reduce_fusion
  212.9 0.7 add_convert_fusion
  (31 shorter events, 0.2 us)
Async XLA Ops:
  7.2 31.6 %copy-start = (bf16[2,1024,256]{2,1,0:T(8,128)(2,1)S(1)}, bf16[2,1024,256]{2,1,0:T(8,128)(2,1)}, u32[]{:S(2)}) copy-start(bf16[2,1024,256]{2,1,0:T(8,128)(2,1)} %param.22) | copy-start | bytes 3145732
  7.2 32.3 %copy-start.12 = (bf16[2,1024,256]{2,1,0:T(8,128)(2,1)S(1)}, bf16[2,1024,256]{2,1,0:T(8,128)(2,1)}, u32[]{:S(2)}) copy-start(bf16[2,1024,256]{2,1,0:T(8,128)(2,1)} %param.23) | copy-start | bytes 3145732
  9.7 15.6 %all-to-all-start = ((bf16[16,2,2048]{2,1,0:T(2,128)(2,1)}), bf16[16,2,2048]{2,1,0:T(2,128)(2,1)S(1)}, u32[]{:S(2)}, u32[]{:S(2)}) async-start(bf16[16,2,2048]{2,1,0:T(2,128)(2,1)} %broadcast_in_dim.37), calls=%async_computation | async-start | bytes 262144 | tf_op jit(solution)/shard_map/all_to_all | solution.py:23
  26.3 20.8 %copy-start.4 = (f32[2,4]{1,0:T(2,128)S(1)}, f32[2,4]{1,0:T(2,128)}, u32[]{:S(2)}) copy-start(f32[2,4]{1,0:T(2,128)} %param.27) | copy-start | bytes 100
  27.6 25.9 %copy-start.2 = (bf16[2048,128]{1,0:T(8,128)(2,1)S(1)}, bf16[2048,128]{1,0:T(8,128)(2,1)}, u32[]{:S(2)}) copy-start(bf16[2048,128]{1,0:T(8,128)(2,1)} %param.33) | copy-start | bytes 1572868
  28.2 10.3 %all-to-all-start.1 = ((bf16[16,2,160]{2,1,0:T(2,128)(2,1)}), bf16[16,2,160]{2,1,0:T(2,128)(2,1)S(1)}, u32[]{:S(2)}, u32[]{:S(2)}) async-start(bf16[16,2,160]{2,1,0:T(2,128)(2,1)} %copy.45), calls=%async_computation.1 | async-start | bytes 32768 | tf_op jit(solution)/shard_map/all_to_all | solution.py:89
  38.6 15.7 %copy-start.7 = (bf16[2,512]{1,0:T(2,128)(2,1)}, bf16[2,512]{1,0:T(2,128)(2,1)S(1)}, u32[]{:S(2)}) copy-start(bf16[2,512]{1,0:T(2,128)(2,1)S(1)} %reshape.145) | copy-start | bytes 6148
  38.8 21.3 %copy-start.9 = (s32[2,4]{1,0:T(2,128)S(1)}, s32[2,4]{1,0:T(2,128)}, u32[]{:S(2)}) copy-start(s32[2,4]{1,0:T(2,128)} %param.26) | copy-start | bytes 100
  38.8 25.6 %copy-start.3 = (bf16[2,2048]{1,0:T(2,128)(2,1)S(1)}, bf16[2,2048]{1,0:T(2,128)(2,1)}, u32[]{:S(2)}) copy-start(bf16[2,2048]{1,0:T(2,128)(2,1)} %param.21) | copy-start | bytes 24580
  38.8 25.6 %copy-start.8 = (f32[2048]{0:T(1024)S(1)}, f32[2048]{0:T(1024)}, u32[]{:S(2)}) copy-start(f32[2048]{0:T(1024)} %param.34) | copy-start | bytes 24580
  38.8 25.8 %copy-start.5 = (f32[2048]{0:T(1024)S(1)}, f32[2048]{0:T(1024)}, u32[]{:S(2)}) copy-start(f32[2048]{0:T(1024)} %param.35) | copy-start | bytes 24580
  39.5 84.2 %copy-start.10 = (f32[1,128]{1,0:T(1,128)S(1)}, f32[1,128]{1,0:T(1,128)}, u32[]{:S(2)}) copy-start(f32[1,128]{1,0:T(1,128)} %param.38) | copy-start | bytes 1540
  40.6 12.9 %all-to-all-start.2 = ((bf16[16,2,2048]{2,1,0:T(2,128)(2,1)}), bf16[16,2,2048]{2,1,0:T(2,128)(2,1)S(1)}, u32[]{:S(2)}, u32[]{:S(2)}) async-start(bf16[16,2,2048]{2,1,0:T(2,128)(2,1)} %broadcast_in_dim.42), calls=%async_computation.2 | async-start | bytes 262144 | tf_op jit(solution)/shard_map/all_to_all | solution.py:23
  54.4 9.9 %all-to-all-start.3 = ((bf16[16,2,128]{2,1,0:T(2,128)(2,1)}), bf16[16,2,128]{2,1,0:T(2,128)(2,1)S(1)}, u32[]{:S(2)}, u32[]{:S(2)}) async-start(bf16[16,2,128]{2,1,0:T(2,128)(2,1)} %bitcast.6), calls=%async_computation.3 | async-start | bytes 16384 | tf_op jit(solution)/shard_map/all_to_all | solution.py:125
  60.1 63.6 %all-gather.3.cloned.1.call-start = ((), (), s32[]{:S(2)}) async-start(), calls=%async_computation.8 | async-start | bytes 2228224 | tf_op jit(solution)/shard_map/all_gather | solution.py:139
  66.1 60.1 %copy-start.11 = (f32[1,128]{1,0:T(1,128)S(1)}, f32[1,128]{1,0:T(1,128)}, u32[]{:S(2)}) copy-start(f32[1,128]{1,0:T(1,128)} %param.39) | copy-start | bytes 1540
  87.5 104.0 %reduce-scatter.2.cloned.1.call-start = ((), (), s32[]{:S(2)}) async-start(), calls=%async_computation.7 | async-start | bytes 2228224 | tf_op jit(solution)/shard_map/reduce_scatter | solution.py:144
  123.7 2.6 %copy-start.1 = (bf16[512,1,2048]{2,0,1:T(8,128)(2,1)S(1)}, bf16[512,1,2048]{2,0,1:T(8,128)(2,1)}, u32[]{:S(2)}) copy-start(bf16[512,1,2048]{2,0,1:T(8,128)(2,1)} %all-gather.3.cloned.1.call-done) | copy-start | bytes 6291460
  130.0 82.8 %copy-start.6 = (f32[2048]{0:T(1024)S(1)}, f32[2048]{0:T(1024)}, u32[]{:S(2)}) copy-start(f32[2048]{0:T(1024)} %param.41) | copy-start | bytes 24580
Sparse Core Ops, SparseCore 0:
  87.6 36.0 all-gather.2
  130.2 61.2 reduce-scatter.1
where the time goes:
time: 221 us; the launch traced here: 220 us
  waiting for transfers between devices  114 us (52%)
  blocking collectives  39.8 us (18%)
  starting transfers between devices  27.3 us (12%)
  between operations  14.3 us (6%)
  matrix products  11.8 us (5%)
  other arithmetic  9.53 us (4%)
  local copies, waits for them, and re-layouts  3.91 us (2%)
    reduce_scatter x1, waiting for transfers between devices, per_device(): lax.psum_scatter(jnp.dot(act, w_down[0], preferred_element_type=jnp.float...  61.4 us
    all_gather x1, waiting for transfers between devices, per_device(): pooled = lax.all_gather(flat, 'tp', axis=0, tiled=True)  36.1 us
    all_to_all x1, blocking collectives, per_device(): lax.all_to_all(outbound, 'ep', split_axis=0, concat_axis=0, tiled=True)  20.5 us
    all_to_all x1, blocking collectives, per_device(): lax.all_to_all(summed.reshape(experts, slots, width), 'ep', split_axis=0,...  19.3 us
    all_to_all x2, starting transfers between devices, sent_to_all(): return lax.all_to_all(copies, axis, split_axis=0, concat_axis=0, tiled=True)  15.7 us
    all_to_all x2, waiting for transfers between devices, sent_to_all(): return lax.all_to_all(copies, axis, split_axis=0, concat_axis=0, tiled=True)  9.28 us
    all_to_all x1, starting transfers between devices, per_device(): lax.all_to_all(gathered, 'tp', split_axis=0, concat_axis=1, tiled=True)  5.75 us
    all_to_all x1, starting transfers between devices, per_device(): lax.all_to_all(projected, 'tp', split_axis=0, concat_axis=1, tiled=True)  5.73 us
  transfers between devices with their start and end apart: 6, of which 6 were waited for; matrix products, arithmetic and copies ran while one was open for 2% of the time, Pallas kernels for 0%

commit v1 on v0

--- a/solution.py
+++ b/solution.py
@@ -136,7 +136,9 @@
     slots = outbound.shape[1]
     arrived = lax.all_to_all(outbound, "ep", split_axis=0, concat_axis=0, tiled=True)
     flat = arrived.reshape(experts * slots, width)
-    pooled = lax.all_gather(flat, "tp", axis=0, tiled=True)
+    pooled = jnp.concatenate(
+        lax.all_to_all(jnp.stack([flat] * lax.axis_size("tp")), "tp", 0, 0), axis=0
+    )
     piece = pooled
     gate = jnp.dot(piece, w_gate[0], preferred_element_type=jnp.float32) + gate_bias[0]
     linear = jnp.dot(piece, w_lin[0], preferred_element_type=jnp.float32) + lin_bias[0]

time: 221 us -> 233 us (1.054)
  blocking collectives: 39.8 us -> 95.7 us
  waiting for transfers between devices: 114 us -> 71.4 us
    all_to_all x0 -> x1, blocking collectives: none -> 56.2 us  [per_device(): lax.all_to_all(jnp.stack([flat] * lax.axis_size('tp')), 'tp', 0, 0)]
    all_gather x1 -> x0, waiting for transfers between devices: 36.1 us -> none  [per_device(): pooled = lax.all_gather(flat, 'tp', axis=0, tiled=True)]
    reduce_scatter x1, waiting for transfers between devices: 61.4 us -> 55.2 us  [per_device(): lax.psum_scatter(jnp.dot(act, w_down[0], preferred_element_type=jnp.float...]
  transfers between devices with their start and end apart: 6 -> 5, of which waited for: 6 -> 5; matrix products, arithmetic and copies ran while one was open for 2% -> 2% of each run, Pallas kernels for 0% -> 0%
where the time goes in v1:
time: 233 us; the launch traced here: 232 us
  blocking collectives  95.7 us (41%)
  waiting for transfers between devices  71.4 us (31%)
  starting transfers between devices  27.3 us (12%)
  between operations  14.3 us (6%)
  matrix products  9.93 us (4%)
  other arithmetic  9.53 us (4%)
  local copies, waits for them, and re-layouts  3.5 us (2%)
    all_to_all x1, blocking collectives, per_device(): lax.all_to_all(jnp.stack([flat] * lax.axis_size('tp')), 'tp', 0, 0)  56.2 us
    reduce_scatter x1, waiting for transfers between devices, per_device(): lax.psum_scatter(jnp.dot(act, w_down[0], preferred_element_type=jnp.float...  55.2 us
    all_to_all x1, blocking collectives, per_device(): lax.all_to_all(outbound, 'ep', split_axis=0, concat_axis=0, tiled=True)  20.5 us
    all_to_all x1, blocking collectives, per_device(): lax.all_to_all(summed.reshape(experts, slots, width), 'ep', split_axis=0,...  19.1 us
    all_to_all x2, starting transfers between devices, sent_to_all(): return lax.all_to_all(copies, axis, split_axis=0, concat_axis=0, tiled=True)  15.7 us
    all_to_all x2, waiting for transfers between devices, sent_to_all(): return lax.all_to_all(copies, axis, split_axis=0, concat_axis=0, tiled=True)  9.28 us
    all_to_all x1, starting transfers between devices, per_device(): lax.all_to_all(gathered, 'tp', split_axis=0, concat_axis=1, tiled=True)  5.75 us
    all_to_all x1, starting transfers between devices, per_device(): lax.all_to_all(projected, 'tp', split_axis=0, concat_axis=1, tiled=True)  5.73 us
  transfers between devices with their start and end apart: 5, of which 5 were waited for; matrix products, arithmetic and copies ran while one was open for 2% of the time, Pallas kernels for 0%

profile of v1, /device:TPU:25, one launch (start us, length us, event | category | flops | bytes accessed | tf_op | source)
XLA Modules:
  0.0 231.7 jit_solution(4501024981146327675)
XLA Ops:
  7.2 0.0 copy-start
  7.2 0.0 copy-start.12
  7.2 1.0 fusion.45
  8.2 0.8 fusion.47
  9.0 0.7 broadcast_in_dim.37
  9.7 9.2 %all-to-all-start = ((bf16[16,2,2048]{2,1,0:T(2,128)(2,1)}), bf16[16,2,2048]{2,1,0:T(2,128)(2,1)S(1)}, u32[]{:S(2)}, u32[]{:S(2)}) async-start(bf16[16,2,2048]{2,1,0:T(2,128)(2,1)} %broadcast_in_dim.37), calls=%async_computation | async-start | bytes 262144 | tf_op jit(solution)/shard_map/all_to_all | solution.py:23
  18.9 0.7 broadcast_add_fusion
  19.5 0.1 iota_compare_fusion
  19.6 0.8 select_reduce_fusion
  20.4 0.8 fusion.55
  21.3 0.8 broadcast_subtract_fusion
  22.1 3.2 %all-to-all-done = bf16[16,2,2048]{2,1,0:T(2,128)(2,1)S(1)} async-done(((bf16[16,2,2048]{2,1,0:T(2,128)(2,1)}), bf16[16,2,2048]{2,1,0:T(2,128)(2,1)S(1)}, u32[]{:S(2)}, u32[]{:S(2)}) %all-to-all-start) | async-done | bytes 131104 | tf_op jit(solution)/shard_map/all_to_all | solution.py:23
  25.2 1.1 convolution_convert_fusion.3
  26.3 0.0 copy-start.4
  26.3 1.3 convolution_convert_fusion.4
  27.6 0.0 copy-start.1
  27.6 0.6 copy.44
  28.2 5.8 %all-to-all-start.1 = ((bf16[16,2,160]{2,1,0:T(2,128)(2,1)}), bf16[16,2,160]{2,1,0:T(2,128)(2,1)S(1)}, u32[]{:S(2)}, u32[]{:S(2)}) async-start(bf16[16,2,160]{2,1,0:T(2,128)(2,1)} %copy.44), calls=%async_computation.1 | async-start | bytes 32768 | tf_op jit(solution)/shard_map/all_to_all | solution.py:89
  34.0 0.7 iota_compare_fusion.1
  34.7 0.8 reduce_max.19
  35.5 3.0 %all-to-all-done.1 = bf16[16,2,160]{2,1,0:T(2,128)(2,1)S(1)} async-done(((bf16[16,2,160]{2,1,0:T(2,128)(2,1)}), bf16[16,2,160]{2,1,0:T(2,128)(2,1)S(1)}, u32[]{:S(2)}, u32[]{:S(2)}) %all-to-all-start.1) | async-done | bytes 10272 | tf_op jit(solution)/shard_map/all_to_all | solution.py:89
  38.5 0.1 reshape.147
  38.7 0.1 fusion.48
  38.8 0.0 copy-done
  38.8 0.0 copy-start.5
  38.8 0.5 fusion.66
  39.3 0.2 fusion.37
  39.5 0.3 fusion.9
  39.8 0.7 broadcast_in_dim.42
  40.6 6.6 %all-to-all-start.2 = ((bf16[16,2,2048]{2,1,0:T(2,128)(2,1)}), bf16[16,2,2048]{2,1,0:T(2,128)(2,1)S(1)}, u32[]{:S(2)}, u32[]{:S(2)}) async-start(bf16[16,2,2048]{2,1,0:T(2,128)(2,1)} %broadcast_in_dim.42), calls=%async_computation.2 | async-start | bytes 262144 | tf_op jit(solution)/shard_map/all_to_all | solution.py:23
  47.1 0.2 fusion.58
  47.3 0.1 fusion.57
  47.4 6.1 %all-to-all-done.2 = bf16[16,2,2048]{2,1,0:T(2,128)(2,1)S(1)} async-done(((bf16[16,2,2048]{2,1,0:T(2,128)(2,1)}), bf16[16,2,2048]{2,1,0:T(2,128)(2,1)S(1)}, u32[]{:S(2)}, u32[]{:S(2)}) %all-to-all-start.2) | async-done | bytes 131104 | tf_op jit(solution)/shard_map/all_to_all | solution.py:23
  53.5 0.1 reshape.150
  53.5 0.8 convolution_convert_fusion.2
  54.3 0.0 copy-done.7
  54.3 5.7 %all-to-all-start.3 = ((bf16[16,2,128]{2,1,0:T(2,128)(2,1)}), bf16[16,2,128]{2,1,0:T(2,128)(2,1)S(1)}, u32[]{:S(2)}, u32[]{:S(2)}) async-start(bf16[16,2,128]{2,1,0:T(2,128)(2,1)} %bitcast.6), calls=%async_computation.3 | async-start | bytes 16384 | tf_op jit(solution)/shard_map/all_to_all | solution.py:125
  60.1 0.0 reduce-scatter.2.cloned.1.call-start
  60.1 0.1 convert_reduce_fusion
  60.2 4.0 %all-to-all-done.3 = bf16[16,2,128]{2,1,0:T(2,128)(2,1)S(1)} async-done(((bf16[16,2,128]{2,1,0:T(2,128)(2,1)}), bf16[16,2,128]{2,1,0:T(2,128)(2,1)S(1)}, u32[]{:S(2)}, u32[]{:S(2)}) %all-to-all-start.3) | async-done | bytes 8224 | tf_op jit(solution)/shard_map/all_to_all | solution.py:125
  64.2 0.1 fusion.44
  64.4 0.0 copy-done.8
  64.4 0.2 multiply_reduce_fusion.1
  64.6 0.2 fusion
  64.8 0.5 broadcast.127
  65.4 0.7 reduce.2
  66.0 0.1 reshape.161
  66.1 20.5 %all_to_all.51 = bf16[32,2,1024]{2,1,0:T(2,128)(2,1)S(1)} all-to-all(bf16[32,2,1024]{2,1,0:T(2,128)(2,1)S(1)} %reshape.161), channel_id=1, replica_groups=mesh['ep'=32,'tp'=16] {'ep'}, dimensions={0} | all-to-all | bytes 262144 | tf_op jit(solution)/shard_map/all_to_all | solution.py:137
  86.6 0.1 reshape.162
  86.7 0.1 copy.90
  86.8 0.2 stack.3
  87.0 0.0 copy-start.2
  87.0 0.0 copy-start.10
  87.0 56.2 %all_to_all.52 = bf16[16,32,2048]{2,1,0:T(8,128)(2,1)S(1)} all-to-all(bf16[16,32,2048]{2,1,0:T(8,128)(2,1)S(1)} %stack.3), channel_id=1, replica_groups=mesh['ep'=32,'tp'=16] {'tp'}, dimensions={0} | all-to-all | bytes 4194304 | tf_op jit(solution)/shard_map/all_to_all | solution.py:140
  143.2 0.7 fusion.1
  144.0 3.8 %convolution_convert_fusion = bf16[512,2048]{1,0:T(8,128)(2,1)} fusion(bf16[512,2048]{1,0:T(8,128)(2,1)S(1)} %bitcast.84, bf16[1,128,2048]{2,1,0:T(8,128)(2,1)} %param.40, bf16[1,2048,128]{2,1,0:T(8,128)(2,1)} %param.37, f32[512,128]{1,0:T(8,128)S(1)} %fusion.1, f32[128]{0:T(128)S(1)} %bitcast.93), kind=kOutput, calls=%fused_computation | convolution fusion | flops 538574848 | bytes 5505536 | tf_op jit(solution)/shard_map/dot_general | solution.py:147
  147.8 0.0 reduce-scatter.2.cloned.1.call-update
  147.8 55.2 %reduce-scatter.2.cloned.1.call-done = bf16[32,2048]{1,0:T(8,128)(2,1)} async-done(((bf16[512,2048]{1,0:T(8,128)(2,1)}), bf16[32,2048]{1,0:T(8,128)(2,1)}) %reduce-scatter.2.cloned.1.call-update) | async-done | bytes 131088 | tf_op jit(solution)/shard_map/reduce_scatter | solution.py:146
  203.0 1.6 reduce.3
  204.5 0.1 reshape.163
  204.6 19.1 %all_to_all.53 = bf16[32,2,1024]{2,1,0:T(2,128)(2,1)S(1)} all-to-all(bf16[32,2,1024]{2,1,0:T(2,128)(2,1)S(1)} %reshape.163), channel_id=1, replica_groups=mesh['ep'=32,'tp'=16] {'ep'}, dimensions={0} | all-to-all | bytes 262144 | tf_op jit(solution)/shard_map/all_to_all | solution.py:152
  223.7 0.1 reshape.164
  223.8 0.3 multiply_reduce_fusion
  224.2 0.7 add_convert_fusion
  (30 shorter events, 0.2 us)
Async XLA Ops:
  7.2 31.6 %copy-start = (bf16[2,1024,256]{2,1,0:T(8,128)(2,1)S(1)}, bf16[2,1024,256]{2,1,0:T(8,128)(2,1)}, u32[]{:S(2)}) copy-start(bf16[2,1024,256]{2,1,0:T(8,128)(2,1)} %param.22) | copy-start | bytes 3145732
  7.2 32.3 %copy-start.12 = (bf16[2,1024,256]{2,1,0:T(8,128)(2,1)S(1)}, bf16[2,1024,256]{2,1,0:T(8,128)(2,1)}, u32[]{:S(2)}) copy-start(bf16[2,1024,256]{2,1,0:T(8,128)(2,1)} %param.23) | copy-start | bytes 3145732
  9.7 15.6 %all-to-all-start = ((bf16[16,2,2048]{2,1,0:T(2,128)(2,1)}), bf16[16,2,2048]{2,1,0:T(2,128)(2,1)S(1)}, u32[]{:S(2)}, u32[]{:S(2)}) async-start(bf16[16,2,2048]{2,1,0:T(2,128)(2,1)} %broadcast_in_dim.37), calls=%async_computation | async-start | bytes 262144 | tf_op jit(solution)/shard_map/all_to_all | solution.py:23
  26.3 20.8 %copy-start.4 = (f32[2,4]{1,0:T(2,128)S(1)}, f32[2,4]{1,0:T(2,128)}, u32[]{:S(2)}) copy-start(f32[2,4]{1,0:T(2,128)} %param.27) | copy-start | bytes 100
  27.6 25.9 %copy-start.1 = (bf16[2048,128]{1,0:T(8,128)(2,1)S(1)}, bf16[2048,128]{1,0:T(8,128)(2,1)}, u32[]{:S(2)}) copy-start(bf16[2048,128]{1,0:T(8,128)(2,1)} %param.33) | copy-start | bytes 1572868
  28.2 10.3 %all-to-all-start.1 = ((bf16[16,2,160]{2,1,0:T(2,128)(2,1)}), bf16[16,2,160]{2,1,0:T(2,128)(2,1)S(1)}, u32[]{:S(2)}, u32[]{:S(2)}) async-start(bf16[16,2,160]{2,1,0:T(2,128)(2,1)} %copy.44), calls=%async_computation.1 | async-start | bytes 32768 | tf_op jit(solution)/shard_map/all_to_all | solution.py:89
  38.6 15.7 %copy-start.7 = (bf16[2,512]{1,0:T(2,128)(2,1)}, bf16[2,512]{1,0:T(2,128)(2,1)S(1)}, u32[]{:S(2)}) copy-start(bf16[2,512]{1,0:T(2,128)(2,1)S(1)} %reshape.147) | copy-start | bytes 6148
  38.8 21.3 %copy-start.9 = (s32[2,4]{1,0:T(2,128)S(1)}, s32[2,4]{1,0:T(2,128)}, u32[]{:S(2)}) copy-start(s32[2,4]{1,0:T(2,128)} %param.26) | copy-start | bytes 100
  38.8 25.6 %copy-start.3 = (bf16[2,2048]{1,0:T(2,128)(2,1)S(1)}, bf16[2,2048]{1,0:T(2,128)(2,1)}, u32[]{:S(2)}) copy-start(bf16[2,2048]{1,0:T(2,128)(2,1)} %param.21) | copy-start | bytes 24580
  38.8 25.6 %copy-start.8 = (f32[2048]{0:T(1024)S(1)}, f32[2048]{0:T(1024)}, u32[]{:S(2)}) copy-start(f32[2048]{0:T(1024)} %param.34) | copy-start | bytes 24580
  38.8 25.8 %copy-start.5 = (f32[2048]{0:T(1024)S(1)}, f32[2048]{0:T(1024)}, u32[]{:S(2)}) copy-start(f32[2048]{0:T(1024)} %param.35) | copy-start | bytes 24580
  40.6 12.9 %all-to-all-start.2 = ((bf16[16,2,2048]{2,1,0:T(2,128)(2,1)}), bf16[16,2,2048]{2,1,0:T(2,128)(2,1)S(1)}, u32[]{:S(2)}, u32[]{:S(2)}) async-start(bf16[16,2,2048]{2,1,0:T(2,128)(2,1)} %broadcast_in_dim.42), calls=%async_computation.2 | async-start | bytes 262144 | tf_op jit(solution)/shard_map/all_to_all | solution.py:23
  54.3 9.9 %all-to-all-start.3 = ((bf16[16,2,128]{2,1,0:T(2,128)(2,1)}), bf16[16,2,128]{2,1,0:T(2,128)(2,1)S(1)}, u32[]{:S(2)}, u32[]{:S(2)}) async-start(bf16[16,2,128]{2,1,0:T(2,128)(2,1)} %bitcast.6), calls=%async_computation.3 | async-start | bytes 16384 | tf_op jit(solution)/shard_map/all_to_all | solution.py:125
  60.1 142.9 %reduce-scatter.2.cloned.1.call-start = ((), (), s32[]{:S(2)}) async-start(), calls=%async_computation.8 | async-start | bytes 2228224 | tf_op jit(solution)/shard_map/reduce_scatter | solution.py:146
  87.0 56.2 %copy-start.2 = (bf16[1,2048,128]{2,1,0:T(8,128)(2,1)S(1)}, bf16[1,2048,128]{2,1,0:T(8,128)(2,1)}, u32[]{:S(2)}) copy-start(bf16[1,2048,128]{2,1,0:T(8,128)(2,1)} %param.36) | copy-start | bytes 1572868
  87.0 56.2 %copy-start.10 = (f32[1,128]{1,0:T(1,128)S(1)}, f32[1,128]{1,0:T(1,128)}, u32[]{:S(2)}) copy-start(f32[1,128]{1,0:T(1,128)} %param.38) | copy-start | bytes 1540
  143.2 0.7 copy-start.11
  147.8 76.4 %copy-start.6 = (f32[2048]{0:T(1024)S(1)}, f32[2048]{0:T(1024)}, u32[]{:S(2)}) copy-start(f32[2048]{0:T(1024)} %param.41) | copy-start | bytes 24580
Sparse Core Ops, SparseCore 0:
  147.9 54.9 reduce-scatter.1
